TPU v7x, 32 devices: a whole 2x2x4 slice. The times are simulated.
32 devices in a mesh: ep: 4 (over y, x), tp: 8 (over z, core).
Axes of the slice: x: 2, y: 2, z: 4, core: 2. Of those that a mesh axis runs over, the one named last changes fastest.
Arguments:
- hidden: bfloat16 [160, 4096], P('ep', 'tp'), may hold values from -6 to 6
- positions: int32 [160], P('ep'), may hold values from 0 to 16383
- ret_state: float32 [160, 16, 128, 128], P('ep', 'tp'), may hold values from -1.5 to 1.5
- query_weight: bfloat16 [4096, 2048], P('ep', 'tp'), may hold values from -0.09375 to 0.09375
- key_weight: bfloat16 [4096, 2048], P('ep', 'tp'), may hold values from -0.09375 to 0.09375
- value_weight: bfloat16 [4096, 2048], P('ep', 'tp'), may hold values from -0.09375 to 0.09375
- gate_weight: bfloat16 [4096, 2048], P('ep', 'tp'), may hold values from -0.09375 to 0.09375
- head_gain: float32 [2048], P('tp'), may hold values from 0.1 to 1.9
- out_weight: bfloat16 [2048, 4096], P(None, 'tp'), may hold values from -0.125 to 0.125
- mix_gain: float32 [4096], replicated, may hold values from 0.1 to 1.9
- ffn_gain: float32 [4096], replicated, may hold values from 0.1 to 1.9
- expert_gate: bfloat16 [8, 4096, 2048], P('ep', None, 'tp'), may hold values from -0.09375 to 0.09375
- expert_up: bfloat16 [8, 4096, 2048], P('ep', None, 'tp'), may hold values from -0.09375 to 0.09375
- expert_down: bfloat16 [8, 2048, 4096], P('ep', None, 'tp'), may hold values from -0.125 to 0.125
- route_ids: int32 [160, 2], P('ep'), may hold values from 0 to 7, as said below
- route_weight: float32 [160, 2], P('ep'), may hold values from 0.25 to 1
Outputs:
- updated: bfloat16 [160, 4096], P('ep', 'tp')
- next_state: float32 [160, 16, 128, 128], P('ep', 'tp')
Inputs may be any that keep to these rules, and one draw needn't show every extreme that they name: `route_ids`: each row names two different experts of one group, the group being the numbers g * 2 to g * 2 + 1; in the rows of one device (aligned blocks of 40 rows) no expert is named more than 10 times, and some expert is named exactly 10 times.
All inputs are finite; a program needn't handle non-finite values.
Results may differ from a plain program's by a relative error of at most 0.014.
Values may be sent and summed in bfloat16 or wider, within the bound.
A program may use at most 64 MiB of HBM per device.

v0:
```python
import jax
import jax.numpy as jnp
from jax import lax
from jax.sharding import PartitionSpec as P

D = 4096
HEADS = 16
HEAD = 128
GROUPS = 4
TOP = 2
epsilon = 1e-06
rope_base = 10000.0


def rms_scale(rows, gain):
    values = rows.astype(jnp.float32)
    factor = lax.rsqrt(jnp.mean(values * values, axis=-1, keepdims=True) + epsilon)
    return (values * factor * gain).astype(jnp.bfloat16)


def log_decay(head_ids):
    return jnp.log(1.0 - 2.0 ** (-5.0 - 5.0 * head_ids.astype(jnp.float32) / (HEADS - 1)))


def rotate(values, positions):
    width = values.shape[-1]
    inverse = 1.0 / rope_base ** (jnp.arange(0, width, 2, dtype=jnp.float32) / width)
    angle = positions.astype(jnp.float32)[:, None, None] * inverse[None, None, :]
    cosine = jnp.cos(angle)
    sine = jnp.sin(angle)
    first = values[..., : width // 2]
    second = values[..., width // 2 :]
    return jnp.concatenate(
        [first * cosine - second * sine, first * sine + second * cosine], axis=-1
    )


def retain(query, key_rows, value_rows, gate_rows, ret_state, positions, head_ids, head_gain):
    batch = query.shape[0]
    heads = head_ids.shape[0]

    def split(array):
        return array.astype(jnp.float32).reshape(batch, heads, HEAD)

    rotated_query = rotate(split(query), positions)
    rotated_key = rotate(split(key_rows), positions) * HEAD ** (-0.5)
    value_heads = split(value_rows)
    decay = jnp.exp(log_decay(head_ids))
    next_state = (
        decay[None, :, None, None] * ret_state
        + rotated_key[..., :, None] * value_heads[..., None, :]
    )
    read = jnp.einsum("bhd,bhde->bhe", rotated_query, next_state, precision=lax.Precision.HIGHEST)
    centered = read - jnp.mean(read, axis=-1, keepdims=True)
    normal = centered * lax.rsqrt(jnp.mean(centered * centered, axis=-1, keepdims=True) + epsilon)
    mixed = (
        normal.reshape(batch, heads * HEAD) * head_gain * jax.nn.silu(gate_rows.astype(jnp.float32))
    )
    return (mixed.astype(jnp.bfloat16), next_state)


def per_device(
    hidden,
    positions,
    ret_state,
    query_weight,
    key_weight,
    value_weight,
    gate_weight,
    head_gain,
    out_weight,
    mix_gain,
    ffn_gain,
    expert_gate,
    expert_up,
    expert_down,
    route_ids,
    route_weight,
):
    own_rows = hidden.shape[0]
    slice_width = hidden.shape[1]
    full_rows = lax.all_gather(hidden, "tp", axis=1, tiled=True)
    normed = rms_scale(full_rows, mix_gain)
    columns = lax.all_to_all(normed, "ep", split_axis=1, concat_axis=0, tiled=True)
    stacked = jnp.concatenate([query_weight, key_weight, value_weight, gate_weight], axis=1)
    width = query_weight.shape[1]
    joined = lax.psum_scatter(
        jnp.dot(columns, stacked, preferred_element_type=jnp.float32),
        "ep",
        scatter_dimension=0,
        tiled=True,
    )
    sums = tuple((joined[:, number * width : (number + 1) * width] for number in range(4)))
    query, key_rows, value_rows, gate_rows = tuple((total.astype(jnp.bfloat16) for total in sums))
    heads_here = query_weight.shape[1] // HEAD
    head_ids = lax.axis_index("tp") * heads_here + jnp.arange(heads_here, dtype=jnp.int32)
    mixed, next_state = retain(
        query, key_rows, value_rows, gate_rows, ret_state, positions, head_ids, head_gain
    )
    projected = jnp.dot(
        lax.all_gather(mixed, "tp", axis=1, tiled=True),
        out_weight,
        preferred_element_type=jnp.float32,
    )
    after = (hidden.astype(jnp.float32) + projected).astype(jnp.bfloat16)
    local_experts = expert_gate.shape[0]
    peers = lax.axis_size("ep")
    experts = local_experts * peers
    group_size = experts // GROUPS
    capacity = 2 * ((own_rows // GROUPS + group_size - 1) // group_size)
    chosen = route_ids.reshape(-1)
    onehot = (chosen[:, None] == jnp.arange(experts, dtype=jnp.int32)[None, :]).astype(jnp.int32)
    ranks = jnp.sum((jnp.cumsum(onehot, axis=0) - 1) * onehot, axis=1)
    send_slot = chosen * capacity + ranks
    slot_count = experts * capacity
    placing = (jnp.arange(slot_count, dtype=jnp.int32)[:, None] == send_slot[None, :]).astype(
        jnp.float32
    )
    token_place = jnp.sum(placing.reshape(slot_count, own_rows, TOP), axis=2).astype(jnp.bfloat16)
    after_float = after.astype(jnp.float32)
    squares = lax.psum(jnp.sum(after_float * after_float, axis=1), "tp")
    gain_slice = lax.dynamic_slice_in_dim(
        ffn_gain, lax.axis_index("tp") * slice_width, slice_width, 0
    )
    factor = lax.rsqrt(squares / D + epsilon)
    scaled = (after_float * factor[:, None] * gain_slice).astype(jnp.bfloat16)
    packed = jnp.dot(token_place, scaled, preferred_element_type=jnp.float32).astype(jnp.bfloat16)
    arrived = lax.all_to_all(
        packed.reshape(peers, local_experts, capacity, scaled.shape[1]),
        "ep",
        split_axis=0,
        concat_axis=2,
        tiled=True,
    )
    arrived = lax.all_gather(arrived, "tp", axis=3, tiled=True)
    arrived = arrived.reshape(local_experts, peers * capacity, D)
    gate = jnp.einsum("emd,edf->emf", arrived, expert_gate, preferred_element_type=jnp.float32)
    lifted = jnp.einsum("emd,edf->emf", arrived, expert_up, preferred_element_type=jnp.float32)
    activated = (jax.nn.silu(gate) * lifted).astype(jnp.bfloat16)
    out_width = expert_down.shape[2]
    result = jnp.einsum(
        "emf,efd->emd",
        lax.all_gather(activated, "tp", axis=2, tiled=True),
        expert_down,
        preferred_element_type=jnp.float32,
    ).astype(jnp.bfloat16)
    back = lax.all_to_all(
        result.reshape(local_experts, peers, capacity, out_width),
        "ep",
        split_axis=1,
        concat_axis=1,
        tiled=True,
    )
    returned_rows = back.reshape(local_experts * peers * capacity, out_width)
    source_row = (
        chosen % local_experts * (peers * capacity) + chosen // local_experts * capacity + ranks
    )
    values = returned_rows[source_row].astype(jnp.float32).reshape(own_rows, TOP, out_width)
    weighted = jnp.sum(values * route_weight[:, :, None], axis=1)
    updated = (after.astype(jnp.float32) + weighted).astype(jnp.bfloat16)
    return (updated, next_state)


def solution(mesh):
    return jax.shard_map(
        per_device,
        mesh=mesh,
        in_specs=(
            P("ep", "tp"),
            P("ep"),
            P("ep", "tp", None, None),
            P("ep", "tp"),
            P("ep", "tp"),
            P("ep", "tp"),
            P("ep", "tp"),
            P("tp"),
            P(None, "tp"),
            P(),
            P(),
            P("ep", None, "tp"),
            P("ep", None, "tp"),
            P("ep", None, "tp"),
            P("ep", None),
            P("ep", None),
        ),
        out_specs=(P("ep", "tp"), P("ep", "tp", None, None)),
        check_vma=False,
    )
```

profile of v0, /device:TPU:0, one launch (start us, length us, event | category | flops | bytes accessed | tf_op | source)
XLA Modules:
  0.0 168.9 jit_solution(997779446454232462)
XLA Ops:
  7.2 0.0 reduce-scatter.4.cloned.1.call-start
  7.2 16.4 %all_gather.12 = bf16[40,4096]{1,0:T(8,128)(2,1)S(1)} all-gather(bf16[40,512]{1,0:T(8,128)(2,1)} %param.16), channel_id=1, replica_groups=mesh['ep'=4,'tp'=8] {'tp'}, dimensions={1}, use_global_device_ids=true | all-gather | bytes 368640 | tf_op jit(solution)/shard_map/all_gather | solution.py:82
  23.6 0.2 fusion.11
  23.8 0.9 fusion.13
  24.7 10.6 %all_to_all.42 = bf16[40,4,1024]{2,0,1:T(8,128)(2,1)S(1)} all-to-all(bf16[40,4,1024]{2,0,1:T(8,128)(2,1)S(1)} %bitcast.48), channel_id=1, replica_groups=mesh['ep'=4,'tp'=8] {'ep'}, dimensions={1} | all-to-all | bytes 655360 | tf_op jit(solution)/shard_map/all_to_all | solution.py:84
  35.3 2.9 %fusion = f32[160,1024]{1,0:T(8,128)} fusion(bf16[160,1024]{1,0:T(8,128)(2,1)S(1)} %bitcast.52, bf16[1024,256]{1,0:T(8,128)(2,1)} %param.22, bf16[1024,256]{1,0:T(8,128)(2,1)} %param.21, bf16[1024,256]{1,0:T(8,128)(2,1)} %param.20, bf16[1024,256]{1,0:T(8,128)(2,1)} %param.19), kind=kOutput, calls=%fused_computation.2 | convolution fusion | flops 343932928 | bytes 3080192 | tf_op jit(solution)/shard_map/dot_general | solution.py:88
  38.2 0.0 reduce-scatter.4.cloned.1.call-update
  38.3 0.1 copy.65
  38.4 0.1 eq.32
  38.5 0.1 reshape.300
  38.6 0.1 fusion.23
  38.7 0.1 reduce_window_sum.11
  38.8 0.2 select_reduce_fusion
  39.0 0.1 reduce_sum.71
  39.1 0.1 copy.66
  39.2 0.8 dynamic_slice.3
  40.0 0.1 convert_reduce_fusion
  40.1 0.2 multiply_cosine_fusion
  40.3 23.2 %reduce-scatter.4.cloned.1.call-done = f32[40,1024]{1,0:T(8,128)} async-done(((f32[160,1024]{1,0:T(8,128)}), f32[40,1024]{1,0:T(8,128)}) %reduce-scatter.4.cloned.1.call-update) | async-done | bytes 163856
  63.4 0.9 convert.10
  64.5 0.2 multiply_subtract_fusion
  64.7 0.2 pad_maximum_fusion
  64.9 4.0 %multiply_add_fusion = f32[40,2,128,128]{3,2,1,0:T(8,128)S(1)} fusion(f32[40,2,128,128]{3,2,1,0:T(8,128)} %param.18, f32[40,2,128]{2,1,0:T(2,128)S(1)} %reshape.305, f32[40,2,128]{2,1,0:T(2,128)S(1)} %get-tuple-element.16, f32[2]{0:T(128)S(1)} %log_exponential_fusion), kind=kLoop, calls=%fused_computation.1 | loop fusion | flops 3932160 | bytes 10567688 | tf_op jit(solution)/shard_map/add | solution.py:50
  68.9 2.3 %copy-done.1 = f32[40,2,128,128]{3,2,1,0:T(8,128)} copy-done((f32[40,2,128,128]{3,2,1,0:T(8,128)}, f32[40,2,128,128]{3,2,1,0:T(8,128)S(1)}, u32[]{:S(2)}) %copy-start.1) | copy-done | bytes 5242904
  71.3 4.5 %fusion.31 = f32[40,2,1,128]{3,2,1,0:T(1,128)S(1)} fusion(f32[40,2,128,1]{2,3,1,0:T(1,128)S(1)} %bitcast.55, f32[40,2,128,128]{3,2,1,0:T(8,128)S(1)} %multiply_add_fusion), kind=kOutput, calls=%fused_computation.78 | convolution fusion | flops 15728640 | bytes 5324800 | tf_op jit(solution)/shard_map/bhd,bhde->bhe/dot_general | solution.py:53
  75.8 0.1 reduce_sum.68
  76.0 0.2 multiply_reduce_fusion.2
  76.2 0.1 subtract_multiply_fusion
  76.4 14.2 %all_gather.13 = bf16[40,2048]{1,0:T(8,128)(2,1)S(1)} all-gather(bf16[40,256]{1,0:T(8,128)(2,1)S(1)} %fusion.24), channel_id=1, replica_groups=mesh['ep'=4,'tp'=8] {'tp'}, dimensions={1}, use_global_device_ids=true | all-gather | bytes 184320 | tf_op jit(solution)/shard_map/all_gather | solution.py:101
  90.5 0.6 multiply_reduce_fusion.1
  91.1 16.8 %psum.7 = f32[40]{0:T(128)S(1)} all-reduce(f32[40]{0:T(128)S(1)} %get-tuple-element.13), channel_id=1, replica_groups=mesh['ep'=4,'tp'=8] {'tp'}, use_global_device_ids=true, to_apply=%region_8.9 | all-reduce | flops 40 | bytes 320 | tf_op jit(solution)/shard_map/psum | solution.py:121
  107.9 0.2 convolution_convert_fusion.1
  108.2 0.7 copy.67
  108.9 3.3 %all-to-all-start.1 = ((bf16[4,2,10,512]{3,1,2,0:T(2,128)(2,1)}), bf16[4,2,10,512]{3,1,2,0:T(2,128)(2,1)S(1)}, u32[]{:S(2)}, u32[]{:S(2)}) async-start(bf16[4,2,10,512]{3,1,2,0:T(2,128)(2,1)} %copy.67), calls=%async_computation.1 | async-start | bytes 163840 | tf_op jit(solution)/shard_map/all_to_all | solution.py:128
  112.2 0.1 copy.72
  112.3 4.7 %all-to-all-done.1 = bf16[4,2,10,512]{3,1,2,0:T(2,128)(2,1)S(1)} async-done(((bf16[4,2,10,512]{3,1,2,0:T(2,128)(2,1)}), bf16[4,2,10,512]{3,1,2,0:T(2,128)(2,1)S(1)}, u32[]{:S(2)}, u32[]{:S(2)}) %all-to-all-start.1) | async-done | bytes 81952 | tf_op jit(solution)/shard_map/all_to_all | solution.py:128
  117.0 15.5 %all_gather.14 = bf16[1,2,40,4096]{3,2,1,0:T(8,128)(2,1)S(1)} all-gather(bf16[1,2,40,512]{3,2,1,0:T(8,128)(2,1)S(1)} %copy.68), channel_id=1, replica_groups=mesh['ep'=4,'tp'=8] {'tp'}, dimensions={3}, use_global_device_ids=true | all-gather | bytes 737280 | tf_op jit(solution)/shard_map/all_gather | solution.py:135
  132.5 2.9 %fusion.15 = f32[2,40,256]{2,1,0:T(8,128)S(1)} fusion(bf16[2,4096,256]{2,1,0:T(8,128)(2,1)} %param.27, bf16[1,2,40,4096]{3,2,1,0:T(8,128)(2,1)S(1)} %all_gather.14), kind=kOutput, calls=%fused_computation.23 | convolution fusion | flops 167772160 | bytes 4931584 | tf_op jit(solution)/shard_map/emd,edf->emf/dot_general | solution.py:137
  135.4 0.7 fusion.8
  136.1 14.4 %all_gather.15 = bf16[2,40,2048]{2,1,0:T(8,128)(2,1)S(1)} all-gather(bf16[2,40,256]{2,1,0:T(8,128)(2,1)S(1)} %fusion.8), channel_id=1, replica_groups=mesh['ep'=4,'tp'=8] {'tp'}, dimensions={2}, use_global_device_ids=true | all-gather | bytes 368640 | tf_op jit(solution)/shard_map/all_gather | solution.py:143
  150.5 0.8 convolution_convert_fusion
  151.3 0.7 copy.69
  152.0 3.3 %all-to-all-start.2 = ((bf16[2,4,10,512]{3,0,2,1:T(2,128)(2,1)}), bf16[2,4,10,512]{3,0,2,1:T(2,128)(2,1)S(1)}, u32[]{:S(2)}, u32[]{:S(2)}) async-start(bf16[2,4,10,512]{3,0,2,1:T(2,128)(2,1)} %bitcast.10), calls=%async_computation.2 | async-start | bytes 163840 | tf_op jit(solution)/shard_map/all_to_all | solution.py:147
  155.4 4.8 %all-to-all-done.2 = bf16[2,4,10,512]{3,0,2,1:T(2,128)(2,1)S(1)} async-done(((bf16[2,4,10,512]{3,0,2,1:T(2,128)(2,1)}), bf16[2,4,10,512]{3,0,2,1:T(2,128)(2,1)S(1)}, u32[]{:S(2)}, u32[]{:S(2)}) %all-to-all-start.2) | async-done | bytes 81952 | tf_op jit(solution)/shard_map/all_to_all | solution.py:147
  160.3 0.7 gather_fusion
  161.0 0.1 reshape.306
  161.1 0.3 multiply_reduce_fusion
  161.4 0.6 add_convert_fusion
  (37 shorter events, 0.4 us)
Async XLA Ops:
  7.2 83.4 %copy-start = (bf16[2048,512]{1,0:T(8,128)(2,1)S(1)}, bf16[2048,512]{1,0:T(8,128)(2,1)}, u32[]{:S(2)}) copy-start(bf16[2048,512]{1,0:T(8,128)(2,1)} %param.24) | copy-start | bytes 6291460
  7.2 56.3 %reduce-scatter.4.cloned.1.call-start = ((), (), s32[]{:S(2)}) async-start(), calls=%async_computation.4 | async-start | bytes 819200
  35.3 2.9 %copy-start.5 = (s32[40,2]{0,1:T(2,128)S(1)}, s32[40,2]{0,1:T(2,128)}, u32[]{:S(2)}) copy-start(s32[40,2]{0,1:T(2,128)} %param.30) | copy-start | bytes 964
  35.3 3.3 %copy-start.8 = (s32[40]{0:T(128)S(1)}, s32[40]{0:T(128)}, u32[]{:S(2)}) copy-start(s32[40]{0:T(128)} %param.17) | copy-start | bytes 484
  68.9 2.4 %copy-start.1 = (f32[40,2,128,128]{3,2,1,0:T(8,128)}, f32[40,2,128,128]{3,2,1,0:T(8,128)S(1)}, u32[]{:S(2)}) copy-start(f32[40,2,128,128]{3,2,1,0:T(8,128)S(1)} %multiply_add_fusion) | copy-start | bytes 15728644
  68.9 7.4 %copy-start.7 = (f32[256]{0:T(256)S(1)}, f32[256]{0:T(256)}, u32[]{:S(2)}) copy-start(f32[256]{0:T(256)} %param.23) | copy-start | bytes 3076
  68.9 21.6 %copy-start.4 = (bf16[40,512]{1,0:T(8,128)(2,1)S(1)}, bf16[40,512]{1,0:T(8,128)(2,1)}, u32[]{:S(2)}) copy-start(bf16[40,512]{1,0:T(8,128)(2,1)} %param.16) | copy-start | bytes 122884
  71.3 40.9 %copy-start.6 = (f32[40,2]{0,1:T(2,128)S(1)}, f32[40,2]{0,1:T(2,128)}, u32[]{:S(2)}) copy-start(f32[40,2]{0,1:T(2,128)} %param.31) | copy-start | bytes 964
  108.9 8.2 %all-to-all-start.1 = ((bf16[4,2,10,512]{3,1,2,0:T(2,128)(2,1)}), bf16[4,2,10,512]{3,1,2,0:T(2,128)(2,1)S(1)}, u32[]{:S(2)}, u32[]{:S(2)}) async-start(bf16[4,2,10,512]{3,1,2,0:T(2,128)(2,1)} %copy.67), calls=%async_computation.1 | async-start | bytes 163840 | tf_op jit(solution)/shard_map/all_to_all | solution.py:128
  117.0 18.4 %copy-start.3 = (bf16[2,4096,256]{2,1,0:T(8,128)(2,1)S(1)}, bf16[2,4096,256]{2,1,0:T(8,128)(2,1)}, u32[]{:S(2)}) copy-start(bf16[2,4096,256]{2,1,0:T(8,128)(2,1)} %param.28) | copy-start | bytes 12582916
  135.4 15.1 %copy-start.2 = (bf16[2,2048,512]{2,1,0:T(8,128)(2,1)S(1)}, bf16[2,2048,512]{2,1,0:T(8,128)(2,1)}, u32[]{:S(2)}) copy-start(bf16[2,2048,512]{2,1,0:T(8,128)(2,1)} %param.29) | copy-start | bytes 12582916
  152.0 8.2 %all-to-all-start.2 = ((bf16[2,4,10,512]{3,0,2,1:T(2,128)(2,1)}), bf16[2,4,10,512]{3,0,2,1:T(2,128)(2,1)S(1)}, u32[]{:S(2)}, u32[]{:S(2)}) async-start(bf16[2,4,10,512]{3,0,2,1:T(2,128)(2,1)} %bitcast.10), calls=%async_computation.2 | async-start | bytes 163840 | tf_op jit(solution)/shard_map/all_to_all | solution.py:147
Sparse Core Ops, SparseCore 0:
  38.4 25.0 reduce-scatter.3
where the time goes:
time: 169 us
  blocking collectives  87.8 us (52%)
  waiting for transfers between devices  32.8 us (19%)
  between operations  14.4 us (9%)
  matrix products  12.6 us (7%)
  other arithmetic  8.45 us (5%)
  starting transfers between devices  6.62 us (4%)
  local copies, waits for them, and re-layouts  6.2 us (4%)
    unnamed x2, waiting for transfers between devices  23.2 us
    psum x1, blocking collectives, per_device(): squares = lax.psum(jnp.sum(after_float * after_float, axis=1), 'tp')  16.8 us
    all_gather x1, blocking collectives, per_device(): full_rows = lax.all_gather(hidden, 'tp', axis=1, tiled=True)  16.4 us
    all_gather x1, blocking collectives, per_device(): arrived = lax.all_gather(arrived, 'tp', axis=3, tiled=True)  15.5 us
    all_gather x1, blocking collectives, per_device(): lax.all_gather(activated, 'tp', axis=2, tiled=True)  14.4 us
    all_gather x1, blocking collectives, per_device(): lax.all_gather(mixed, 'tp', axis=1, tiled=True)  14.2 us
    all_to_all x1, blocking collectives, per_device(): lax.all_to_all(normed, 'ep', split_axis=1, concat_axis=0, tiled=True)  10.6 us
    all_to_all x1, waiting for transfers between devices, per_device(): lax.all_to_all(result.reshape(local_experts, peers, capacity, out_width),...  4.84 us
  transfers between devices with their start and end apart: 3, of which 3 were waited for; matrix products, arithmetic and copies ran while one was open for 1% of the time, Pallas kernels for 0%

commit v1 on v0

--- a/solution.py
+++ b/solution.py
@@ -138,11 +138,28 @@
     lifted = jnp.einsum("emd,edf->emf", arrived, expert_up, preferred_element_type=jnp.float32)
     activated = (jax.nn.silu(gate) * lifted).astype(jnp.bfloat16)
     out_width = expert_down.shape[2]
-    result = jnp.einsum(
-        "emf,efd->emd",
-        lax.all_gather(activated, "tp", axis=2, tiled=True),
-        expert_down,
-        preferred_element_type=jnp.float32,
+
+    def define_pipes(state, u_in):
+        before = lax.axis_size("tp")
+        response = lax.axis_index("tp")
+        w_next, long_array = (before, response)
+        sheets = tuple(((dev_i, (dev_i - 1) % w_next) for dev_i in range(w_next)))
+        next_value = state.shape[2]
+        parts_out = state
+        state_next = u_in(parts_out, long_array * next_value)
+        for nth in range(1, w_next):
+            parts_out = lax.ppermute(parts_out, "tp", sheets)
+            state_next = state_next + u_in(parts_out, (long_array + nth) % w_next * next_value)
+        return state_next
+
+    result = define_pipes(
+        activated,
+        lambda part, offset: jnp.einsum(
+            "emf,efd->emd",
+            part,
+            lax.dynamic_slice_in_dim(expert_down, offset, part.shape[2], axis=1),
+            preferred_element_type=jnp.float32,
+        ),
     ).astype(jnp.bfloat16)
     back = lax.all_to_all(
         result.reshape(local_experts, peers, capacity, out_width),

time: 169 us -> 188 us (1.11)
  starting transfers between devices: 6.62 us -> 28.6 us
  blocking collectives: 87.8 us -> 73.4 us
  waiting for transfers between devices: 32.8 us -> 42.2 us
    ppermute x0 -> x7, starting transfers between devices: none -> 22 us  [define_pipes(): parts_out = lax.ppermute(parts_out, 'tp', sheets)]
    all_gather x1 -> x0, blocking collectives: 14.4 us -> none  [per_device(): lax.all_gather(activated, 'tp', axis=2, tiled=True)]
    ppermute x0 -> x7, waiting for transfers between devices: none -> 9.49 us  [define_pipes(): parts_out = lax.ppermute(parts_out, 'tp', sheets)]
  transfers between devices with their start and end apart: 3 -> 10, of which waited for: 3 -> 10; matrix products, arithmetic and copies ran while one was open for 1% -> 2% of each run, Pallas kernels for 0% -> 0%
where the time goes in v1:
time: 188 us
  blocking collectives  73.4 us (39%)
  waiting for transfers between devices  42.2 us (22%)
  starting transfers between devices  28.6 us (15%)
  between operations  14.5 us (8%)
  matrix products  13.4 us (7%)
  other arithmetic  8.47 us (5%)
  local copies, waits for them, and re-layouts  6.99 us (4%)
    unnamed x2, waiting for transfers between devices  23.2 us
    ppermute x7, starting transfers between devices, define_pipes(): parts_out = lax.ppermute(parts_out, 'tp', sheets)  22 us
    psum x1, blocking collectives, per_device(): squares = lax.psum(jnp.sum(after_float * after_float, axis=1), 'tp')  16.8 us
    all_gather x1, blocking collectives, per_device(): full_rows = lax.all_gather(hidden, 'tp', axis=1, tiled=True)  16.4 us
    all_gather x1, blocking collectives, per_device(): arrived = lax.all_gather(arrived, 'tp', axis=3, tiled=True)  15.5 us
    all_gather x1, blocking collectives, per_device(): lax.all_gather(mixed, 'tp', axis=1, tiled=True)  14.2 us
    all_to_all x1, blocking collectives, per_device(): lax.all_to_all(normed, 'ep', split_axis=1, concat_axis=0, tiled=True)  10.6 us
    ppermute x7, waiting for transfers between devices, define_pipes(): parts_out = lax.ppermute(parts_out, 'tp', sheets)  9.49 us
  transfers between devices with their start and end apart: 10, of which 10 were waited for; matrix products, arithmetic and copies ran while one was open for 2% of the time, Pallas kernels for 0%

profile of v1, /device:TPU:0, one launch (start us, length us, event | category | flops | bytes accessed | tf_op | source)
XLA Modules:
  0.0 187.5 jit_solution(10967369341184386399)
XLA Ops:
  7.2 16.4 %all_gather.9 = bf16[40,4096]{1,0:T(8,128)(2,1)S(1)} all-gather(bf16[40,512]{1,0:T(8,128)(2,1)} %param.16), channel_id=1, replica_groups=mesh['ep'=4,'tp'=8] {'tp'}, dimensions={1}, use_global_device_ids=true | all-gather | bytes 368640 | tf_op jit(solution)/shard_map/all_gather | solution.py:82
  23.8 0.9 fusion.14
  24.7 10.6 %all_to_all.42 = bf16[40,4,1024]{2,0,1:T(8,128)(2,1)S(1)} all-to-all(bf16[40,4,1024]{2,0,1:T(8,128)(2,1)S(1)} %bitcast.54), channel_id=1, replica_groups=mesh['ep'=4,'tp'=8] {'ep'}, dimensions={1} | all-to-all | bytes 655360 | tf_op jit(solution)/shard_map/all_to_all | solution.py:84
  35.3 2.9 %fusion = f32[160,1024]{1,0:T(8,128)} fusion(bf16[160,1024]{1,0:T(8,128)(2,1)S(1)} %bitcast.58, bf16[1024,256]{1,0:T(8,128)(2,1)} %param.22, bf16[1024,256]{1,0:T(8,128)(2,1)} %param.21, bf16[1024,256]{1,0:T(8,128)(2,1)} %param.20, bf16[1024,256]{1,0:T(8,128)(2,1)} %param.19), kind=kOutput, calls=%fused_computation.2 | convolution fusion | flops 343932928 | bytes 3080192 | tf_op jit(solution)/shard_map/dot_general | solution.py:88
  39.2 0.8 dynamic_slice.27
  40.3 23.2 %reduce-scatter.4.cloned.1.call-done = f32[40,1024]{1,0:T(8,128)} async-done(((f32[160,1024]{1,0:T(8,128)}), f32[40,1024]{1,0:T(8,128)}) %reduce-scatter.4.cloned.1.call-update) | async-done | bytes 163856
  63.4 0.9 convert.10
  64.5 0.2 multiply_subtract_fusion
  64.9 4.1 %multiply_add_fusion = f32[40,2,128,128]{3,2,1,0:T(8,128)S(1)} fusion(f32[40,2,128,128]{3,2,1,0:T(8,128)} %param.18, f32[40,2,128]{2,1,0:T(2,128)S(1)} %reshape.305, f32[40,2,128]{2,1,0:T(2,128)S(1)} %get-tuple-element.16, f32[2]{0:T(128)S(1)} %log_exponential_fusion), kind=kLoop, calls=%fused_computation.1 | loop fusion | flops 3932160 | bytes 10567688 | tf_op jit(solution)/shard_map/add | solution.py:50
  69.0 2.3 %copy-done.1 = f32[40,2,128,128]{3,2,1,0:T(8,128)} copy-done((f32[40,2,128,128]{3,2,1,0:T(8,128)}, f32[40,2,128,128]{3,2,1,0:T(8,128)S(1)}, u32[]{:S(2)}) %copy-start.1) | copy-done | bytes 5242904
  71.3 4.5 %fusion.49 = f32[40,2,1,128]{3,2,1,0:T(1,128)S(1)} fusion(f32[40,2,128,1]{2,3,1,0:T(1,128)S(1)} %bitcast.61, f32[40,2,128,128]{3,2,1,0:T(8,128)S(1)} %multiply_add_fusion), kind=kOutput, calls=%fused_computation.102 | convolution fusion | flops 15728640 | bytes 5324800 | tf_op jit(solution)/shard_map/bhd,bhde->bhe/dot_general | solution.py:53
  76.4 14.2 %all_gather.10 = bf16[40,2048]{1,0:T(8,128)(2,1)S(1)} all-gather(bf16[40,256]{1,0:T(8,128)(2,1)S(1)} %fusion.34), channel_id=1, replica_groups=mesh['ep'=4,'tp'=8] {'tp'}, dimensions={1}, use_global_device_ids=true | all-gather | bytes 184320 | tf_op jit(solution)/shard_map/all_gather | solution.py:101
  90.5 0.6 multiply_reduce_fusion.1
  91.1 16.8 %psum.7 = f32[40]{0:T(128)S(1)} all-reduce(f32[40]{0:T(128)S(1)} %get-tuple-element.13), channel_id=1, replica_groups=mesh['ep'=4,'tp'=8] {'tp'}, use_global_device_ids=true, to_apply=%region_8.9 | all-reduce | flops 40 | bytes 320 | tf_op jit(solution)/shard_map/psum | solution.py:121
  107.9 0.2 convolution_convert_fusion
  108.2 0.7 copy.67
  108.9 3.3 %all-to-all-start.1 = ((bf16[4,2,10,512]{3,1,2,0:T(2,128)(2,1)}), bf16[4,2,10,512]{3,1,2,0:T(2,128)(2,1)S(1)}, u32[]{:S(2)}, u32[]{:S(2)}) async-start(bf16[4,2,10,512]{3,1,2,0:T(2,128)(2,1)} %copy.67), calls=%async_computation.1 | async-start | bytes 163840 | tf_op jit(solution)/shard_map/all_to_all | solution.py:128
  112.4 4.6 %all-to-all-done.1 = bf16[4,2,10,512]{3,1,2,0:T(2,128)(2,1)S(1)} async-done(((bf16[4,2,10,512]{3,1,2,0:T(2,128)(2,1)}), bf16[4,2,10,512]{3,1,2,0:T(2,128)(2,1)S(1)}, u32[]{:S(2)}, u32[]{:S(2)}) %all-to-all-start.1) | async-done | bytes 81952 | tf_op jit(solution)/shard_map/all_to_all | solution.py:128
  117.0 15.5 %all_gather.11 = bf16[1,2,40,4096]{3,2,1,0:T(8,128)(2,1)S(1)} all-gather(bf16[1,2,40,512]{3,2,1,0:T(8,128)(2,1)S(1)} %copy.68), channel_id=1, replica_groups=mesh['ep'=4,'tp'=8] {'tp'}, dimensions={3}, use_global_device_ids=true | all-gather | bytes 737280 | tf_op jit(solution)/shard_map/all_gather | solution.py:135
  132.5 2.9 %fusion.16 = f32[2,40,256]{2,1,0:T(8,128)S(1)} fusion(bf16[2,4096,256]{2,1,0:T(8,128)(2,1)} %param.27, bf16[1,2,40,4096]{3,2,1,0:T(8,128)(2,1)S(1)} %all_gather.11), kind=kOutput, calls=%fused_computation.30 | convolution fusion | flops 167772160 | bytes 4931584 | tf_op jit(solution)/shard_map/emd,edf->emf/dot_general | solution.py:137
  135.4 0.7 fusion.9
  136.1 0.7 collective-permute-start
  136.8 0.8 copy-done.2
  137.8 0.7 collective-permute-done
  138.5 3.5 %collective-permute-start.1 = (bf16[2,40,256]{2,1,0:T(8,128)(2,1)S(1)}, bf16[2,40,256]{2,1,0:T(8,128)(2,1)S(1)}, u32[]{:S(2)}, u32[]{:S(2)}) collective-permute-start(bf16[2,40,256]{2,1,0:T(8,128)(2,1)S(1)} %collective-permute-done), channel_id=1, source_target_pairs={{0,7},{1,0},{2,1},{3,2},{4,3},{5,4},{6,5},{7,6},{8,15},{9,8},{10,9... | collective-permute-start | bytes 122888 | tf_op jit(solution)/shard_map/ppermute | solution.py:151
  142.0 0.2 convolution_add_fusion.6
  142.2 1.5 collective-permute-done.1
  143.7 3.5 %collective-permute-start.2 = (bf16[2,40,256]{2,1,0:T(8,128)(2,1)S(1)}, bf16[2,40,256]{2,1,0:T(8,128)(2,1)S(1)}, u32[]{:S(2)}, u32[]{:S(2)}) collective-permute-start(bf16[2,40,256]{2,1,0:T(8,128)(2,1)S(1)} %collective-permute-done.1), channel_id=1, source_target_pairs={{0,7},{1,0},{2,1},{3,2},{4,3},{5,4},{6,5},{7,6},{8,15},{9,8},{10,9... | collective-permute-start | bytes 122888 | tf_op jit(solution)/shard_map/ppermute | solution.py:151
  147.2 0.2 convolution_add_fusion.5
  147.4 1.5 collective-permute-done.2
  148.9 3.5 %collective-permute-start.3 = (bf16[2,40,256]{2,1,0:T(8,128)(2,1)S(1)}, bf16[2,40,256]{2,1,0:T(8,128)(2,1)S(1)}, u32[]{:S(2)}, u32[]{:S(2)}) collective-permute-start(bf16[2,40,256]{2,1,0:T(8,128)(2,1)S(1)} %collective-permute-done.2), channel_id=1, source_target_pairs={{0,7},{1,0},{2,1},{3,2},{4,3},{5,4},{6,5},{7,6},{8,15},{9,8},{10,9... | collective-permute-start | bytes 122888 | tf_op jit(solution)/shard_map/ppermute | solution.py:151
  152.5 0.2 convolution_add_fusion.4
  152.7 1.5 collective-permute-done.3
  154.1 3.5 %collective-permute-start.4 = (bf16[2,40,256]{2,1,0:T(8,128)(2,1)S(1)}, bf16[2,40,256]{2,1,0:T(8,128)(2,1)S(1)}, u32[]{:S(2)}, u32[]{:S(2)}) collective-permute-start(bf16[2,40,256]{2,1,0:T(8,128)(2,1)S(1)} %collective-permute-done.3), channel_id=1, source_target_pairs={{0,7},{1,0},{2,1},{3,2},{4,3},{5,4},{6,5},{7,6},{8,15},{9,8},{10,9... | collective-permute-start | bytes 122888 | tf_op jit(solution)/shard_map/ppermute | solution.py:151
  157.7 0.2 convolution_add_fusion.3
  157.9 1.5 collective-permute-done.4
  159.4 3.5 %collective-permute-start.5 = (bf16[2,40,256]{2,1,0:T(8,128)(2,1)S(1)}, bf16[2,40,256]{2,1,0:T(8,128)(2,1)S(1)}, u32[]{:S(2)}, u32[]{:S(2)}) collective-permute-start(bf16[2,40,256]{2,1,0:T(8,128)(2,1)S(1)} %collective-permute-done.4), channel_id=1, source_target_pairs={{0,7},{1,0},{2,1},{3,2},{4,3},{5,4},{6,5},{7,6},{8,15},{9,8},{10,9... | collective-permute-start | bytes 122888 | tf_op jit(solution)/shard_map/ppermute | solution.py:151
  162.9 0.2 convolution_add_fusion.2
  163.1 1.5 collective-permute-done.5
  164.6 3.5 %collective-permute-start.6 = (bf16[2,40,256]{2,1,0:T(8,128)(2,1)S(1)}, bf16[2,40,256]{2,1,0:T(8,128)(2,1)S(1)}, u32[]{:S(2)}, u32[]{:S(2)}) collective-permute-start(bf16[2,40,256]{2,1,0:T(8,128)(2,1)S(1)} %collective-permute-done.5), channel_id=1, source_target_pairs={{0,7},{1,0},{2,1},{3,2},{4,3},{5,4},{6,5},{7,6},{8,15},{9,8},{10,9... | collective-permute-start | bytes 122888 | tf_op jit(solution)/shard_map/ppermute | solution.py:151
  168.1 0.2 convolution_add_fusion.1
  168.3 1.5 collective-permute-done.6
  170.0 0.7 copy.69
  170.7 3.3 %all-to-all-start.2 = ((bf16[2,4,10,512]{3,0,2,1:T(2,128)(2,1)}), bf16[2,4,10,512]{3,0,2,1:T(2,128)(2,1)S(1)}, u32[]{:S(2)}, u32[]{:S(2)}) async-start(bf16[2,4,10,512]{3,0,2,1:T(2,128)(2,1)} %bitcast.10), calls=%async_computation.2 | async-start | bytes 163840 | tf_op jit(solution)/shard_map/all_to_all | solution.py:164
  174.0 4.8 %all-to-all-done.2 = bf16[2,4,10,512]{3,0,2,1:T(2,128)(2,1)S(1)} async-done(((bf16[2,4,10,512]{3,0,2,1:T(2,128)(2,1)}), bf16[2,4,10,512]{3,0,2,1:T(2,128)(2,1)S(1)}, u32[]{:S(2)}, u32[]{:S(2)}) %all-to-all-start.2) | async-done | bytes 81952 | tf_op jit(solution)/shard_map/all_to_all | solution.py:164
  178.9 0.7 gather_fusion
  179.8 0.3 multiply_reduce_fusion
  180.1 0.6 add_convert_fusion
  (57 shorter events, 2.9 us)
Async XLA Ops:
  7.2 83.4 %copy-start = (bf16[2048,512]{1,0:T(8,128)(2,1)S(1)}, bf16[2048,512]{1,0:T(8,128)(2,1)}, u32[]{:S(2)}) copy-start(bf16[2048,512]{1,0:T(8,128)(2,1)} %param.24) | copy-start | bytes 6291460
  7.2 56.3 %reduce-scatter.4.cloned.1.call-start = ((), (), s32[]{:S(2)}) async-start(), calls=%async_computation.4 | async-start | bytes 819200
  35.3 2.9 %copy-start.5 = (s32[40,2]{0,1:T(2,128)S(1)}, s32[40,2]{0,1:T(2,128)}, u32[]{:S(2)}) copy-start(s32[40,2]{0,1:T(2,128)} %param.30) | copy-start | bytes 964
  35.3 3.3 %copy-start.8 = (s32[40]{0:T(128)S(1)}, s32[40]{0:T(128)}, u32[]{:S(2)}) copy-start(s32[40]{0:T(128)} %param.17) | copy-start | bytes 484
  68.9 2.4 %copy-start.1 = (f32[40,2,128,128]{3,2,1,0:T(8,128)}, f32[40,2,128,128]{3,2,1,0:T(8,128)S(1)}, u32[]{:S(2)}) copy-start(f32[40,2,128,128]{3,2,1,0:T(8,128)S(1)} %multiply_add_fusion) | copy-start | bytes 15728644
  68.9 7.4 %copy-start.7 = (f32[256]{0:T(256)S(1)}, f32[256]{0:T(256)}, u32[]{:S(2)}) copy-start(f32[256]{0:T(256)} %param.23) | copy-start | bytes 3076
  68.9 21.6 %copy-start.4 = (bf16[40,512]{1,0:T(8,128)(2,1)S(1)}, bf16[40,512]{1,0:T(8,128)(2,1)}, u32[]{:S(2)}) copy-start(bf16[40,512]{1,0:T(8,128)(2,1)} %param.16) | copy-start | bytes 122884
  71.3 41.0 %copy-start.6 = (f32[40,2]{0,1:T(2,128)S(1)}, f32[40,2]{0,1:T(2,128)}, u32[]{:S(2)}) copy-start(f32[40,2]{0,1:T(2,128)} %param.31) | copy-start | bytes 964
  108.9 8.2 %all-to-all-start.1 = ((bf16[4,2,10,512]{3,1,2,0:T(2,128)(2,1)}), bf16[4,2,10,512]{3,1,2,0:T(2,128)(2,1)S(1)}, u32[]{:S(2)}, u32[]{:S(2)}) async-start(bf16[4,2,10,512]{3,1,2,0:T(2,128)(2,1)} %copy.67), calls=%async_computation.1 | async-start | bytes 163840 | tf_op jit(solution)/shard_map/all_to_all | solution.py:128
  117.0 18.4 %copy-start.3 = (bf16[2,4096,256]{2,1,0:T(8,128)(2,1)S(1)}, bf16[2,4096,256]{2,1,0:T(8,128)(2,1)}, u32[]{:S(2)}) copy-start(bf16[2,4096,256]{2,1,0:T(8,128)(2,1)} %param.28) | copy-start | bytes 12582916
  135.4 2.2 %copy-start.2 = (bf16[2,2048,512]{2,1,0:T(8,128)(2,1)S(1)}, bf16[2,2048,512]{2,1,0:T(8,128)(2,1)}, u32[]{:S(2)}) copy-start(bf16[2,2048,512]{2,1,0:T(8,128)(2,1)} %param.29) | copy-start | bytes 12582916
  136.1 2.3 %collective-permute-start = (bf16[2,40,256]{2,1,0:T(8,128)(2,1)S(1)}, bf16[2,40,256]{2,1,0:T(8,128)(2,1)S(1)}, u32[]{:S(2)}, u32[]{:S(2)}) collective-permute-start(bf16[2,40,256]{2,1,0:T(8,128)(2,1)S(1)} %fusion.9), channel_id=1, source_target_pairs={{0,7},{1,0},{2,1},{3,2},{4,3},{5,4},{6,5},{7,6},{8,15},{9,8},{10,9... | collective-permute-start | bytes 122888 | tf_op jit(solution)/shard_map/ppermute | solution.py:151
  138.5 5.2 %collective-permute-start.1 = (bf16[2,40,256]{2,1,0:T(8,128)(2,1)S(1)}, bf16[2,40,256]{2,1,0:T(8,128)(2,1)S(1)}, u32[]{:S(2)}, u32[]{:S(2)}) collective-permute-start(bf16[2,40,256]{2,1,0:T(8,128)(2,1)S(1)} %collective-permute-done), channel_id=1, source_target_pairs={{0,7},{1,0},{2,1},{3,2},{4,3},{5,4},{6,5},{7,6},{8,15},{9,8},{10,9... | collective-permute-start | bytes 122888 | tf_op jit(solution)/shard_map/ppermute | solution.py:151
  143.7 5.2 %collective-permute-start.2 = (bf16[2,40,256]{2,1,0:T(8,128)(2,1)S(1)}, bf16[2,40,256]{2,1,0:T(8,128)(2,1)S(1)}, u32[]{:S(2)}, u32[]{:S(2)}) collective-permute-start(bf16[2,40,256]{2,1,0:T(8,128)(2,1)S(1)} %collective-permute-done.1), channel_id=1, source_target_pairs={{0,7},{1,0},{2,1},{3,2},{4,3},{5,4},{6,5},{7,6},{8,15},{9,8},{10,9... | collective-permute-start | bytes 122888 | tf_op jit(solution)/shard_map/ppermute | solution.py:151
  148.9 5.2 %collective-permute-start.3 = (bf16[2,40,256]{2,1,0:T(8,128)(2,1)S(1)}, bf16[2,40,256]{2,1,0:T(8,128)(2,1)S(1)}, u32[]{:S(2)}, u32[]{:S(2)}) collective-permute-start(bf16[2,40,256]{2,1,0:T(8,128)(2,1)S(1)} %collective-permute-done.2), channel_id=1, source_target_pairs={{0,7},{1,0},{2,1},{3,2},{4,3},{5,4},{6,5},{7,6},{8,15},{9,8},{10,9... | collective-permute-start | bytes 122888 | tf_op jit(solution)/shard_map/ppermute | solution.py:151
  154.1 5.2 %collective-permute-start.4 = (bf16[2,40,256]{2,1,0:T(8,128)(2,1)S(1)}, bf16[2,40,256]{2,1,0:T(8,128)(2,1)S(1)}, u32[]{:S(2)}, u32[]{:S(2)}) collective-permute-start(bf16[2,40,256]{2,1,0:T(8,128)(2,1)S(1)} %collective-permute-done.3), channel_id=1, source_target_pairs={{0,7},{1,0},{2,1},{3,2},{4,3},{5,4},{6,5},{7,6},{8,15},{9,8},{10,9... | collective-permute-start | bytes 122888 | tf_op jit(solution)/shard_map/ppermute | solution.py:151
  159.4 5.2 %collective-permute-start.5 = (bf16[2,40,256]{2,1,0:T(8,128)(2,1)S(1)}, bf16[2,40,256]{2,1,0:T(8,128)(2,1)S(1)}, u32[]{:S(2)}, u32[]{:S(2)}) collective-permute-start(bf16[2,40,256]{2,1,0:T(8,128)(2,1)S(1)} %collective-permute-done.4), channel_id=1, source_target_pairs={{0,7},{1,0},{2,1},{3,2},{4,3},{5,4},{6,5},{7,6},{8,15},{9,8},{10,9... | collective-permute-start | bytes 122888 | tf_op jit(solution)/shard_map/ppermute | solution.py:151
  164.6 5.2 %collective-permute-start.6 = (bf16[2,40,256]{2,1,0:T(8,128)(2,1)S(1)}, bf16[2,40,256]{2,1,0:T(8,128)(2,1)S(1)}, u32[]{:S(2)}, u32[]{:S(2)}) collective-permute-start(bf16[2,40,256]{2,1,0:T(8,128)(2,1)S(1)} %collective-permute-done.5), channel_id=1, source_target_pairs={{0,7},{1,0},{2,1},{3,2},{4,3},{5,4},{6,5},{7,6},{8,15},{9,8},{10,9... | collective-permute-start | bytes 122888 | tf_op jit(solution)/shard_map/ppermute | solution.py:151
  170.7 8.2 %all-to-all-start.2 = ((bf16[2,4,10,512]{3,0,2,1:T(2,128)(2,1)}), bf16[2,4,10,512]{3,0,2,1:T(2,128)(2,1)S(1)}, u32[]{:S(2)}, u32[]{:S(2)}) async-start(bf16[2,4,10,512]{3,0,2,1:T(2,128)(2,1)} %bitcast.10), calls=%async_computation.2 | async-start | bytes 163840 | tf_op jit(solution)/shard_map/all_to_all | solution.py:164
Sparse Core Ops, SparseCore 0:
  38.4 25.0 reduce-scatter.3
